TPU v7x, 256 devices: a whole 4x4x8 slice. The times are simulated.
256 devices in a mesh: sp: 16 (over y, x), tp: 16 (over z, core).
Axes of the slice: x: 4, y: 4, z: 8, core: 2. Of those that a mesh axis runs over, the one named last changes fastest.
Arguments:
- queries: bfloat16 [8192, 2048], P('sp', 'tp'), may hold values from -16 to 16
- key_vectors: bfloat16 [8192, 2048], P('sp', 'tp'), may hold values from -4 to 4
- value_vectors: bfloat16 [8192, 2048], P('sp', 'tp'), may hold values from -5 to 5
- forget_totals: float32 [8192, 16], P('sp', 'tp'), may hold values from -1368 to 0, as said below
- head_gain: float32 [2048], P('tp'), may hold values from 0.1 to 1.9
- stream: bfloat16 [8192, 2048], P(('sp', 'tp')), may hold values from -6 to 6
- out_weight: bfloat16 [2048, 2048], replicated, may hold values from -0.125 to 0.125
- norm_gain: float32 [2048], replicated, may hold values from 0.1 to 1.9
- routing: int32 [8192, 2], P(('sp', 'tp')), may hold values from 0 to 15, all different within a row; in each aligned block of 32 rows (0 to 31, 32 to 63, ...) at most 8 rows name the same one
- route_weights: float32 [8192, 2], P(('sp', 'tp')), may hold values from 0.2 to 1
- gate_weight: bfloat16 [16, 2048, 4096], P('sp', None, 'tp'), may hold values from -0.125 to 0.125
- up_weight: bfloat16 [16, 2048, 4096], P('sp', None, 'tp'), may hold values from -0.125 to 0.125
- down_weight: bfloat16 [16, 4096, 2048], P('sp', 'tp'), may hold values from -0.09375 to 0.09375
Outputs:
- layer_out: bfloat16 [8192, 2048], P(('sp', 'tp'))
Inputs may be any that keep to these rules, and one draw needn't show every extreme that they name: `forget_totals`: along the positions, the values of each head never rise. `routing`: A token's 2 experts differ. Within the tokens of one device (aligned blocks of 32 rows) no expert is named more than 8 times.
All inputs are finite; a program needn't handle non-finite values.
Results may differ from a plain program's by a relative error of at most 0.01145.
Values may be sent and summed in bfloat16 or wider, within the bound.
A program may use at most 128 MiB of HBM per device.

v0:
```python
from functools import partial
import jax
import jax.numpy as jnp
from jax import lax
from jax.sharding import PartitionSpec as P

HD = 128
TOP = 2
masked_score = -1e30


def sent_together(arrays, axis, dim, along):
    ends, at = ([], 0)
    for a in arrays[:-1]:
        at += a.shape[along]
        ends.append(at)
    both = jnp.concatenate(arrays, axis=along)
    return tuple(jnp.split(lax.all_gather(both, axis, axis=dim, tiled=True), ends, axis=along))


def attend_block(
    totals, query_rows, query_gate, query_pos, key_rows, value_rows, key_gate, key_pos
):
    run_max, run_sum, run_acc = totals
    scores = jnp.einsum("qhd,khd->hqk", query_rows, key_rows, preferred_element_type=jnp.float32)
    scores = scores * HD ** (-0.5) + query_gate[:, :, None] - key_gate[:, None, :]
    visible = (key_pos[None, :] <= query_pos[:, None])[None]
    scores = jnp.where(visible, scores, masked_score)
    new_max = jnp.maximum(run_max, jnp.max(scores, axis=2))
    lifted = jnp.where(visible, jnp.exp(scores - new_max[:, :, None]), 0.0)
    rescale = jnp.exp(run_max - new_max)
    new_sum = run_sum * rescale + jnp.sum(lifted, axis=2)
    product = jnp.einsum(
        "hqk,khd->hqd", lifted.astype(jnp.bfloat16), value_rows, preferred_element_type=jnp.float32
    )
    new_acc = run_acc * rescale[:, :, None] + product
    return (new_max, new_sum, new_acc)


def keep_totals(totals_in):
    return totals_in


def make_folder(segments, gathered_gates):

    def fold_keys(state_all, key_piece, first_key):
        key_part, value_part = key_piece
        key_total = key_part.shape[0]
        block_len = min(512, key_total)
        heads_dev = segments[0][0].shape[1]
        key_part = key_part.reshape(key_total, heads_dev, HD)
        value_part = value_part.reshape(key_total, heads_dev, HD)

        def one_block(block_index, state_now):
            offset = block_index * block_len
            key_rows = lax.dynamic_slice_in_dim(key_part, offset, block_len, 0)
            value_rows = lax.dynamic_slice_in_dim(value_part, offset, block_len, 0)
            key_pos = offset + jnp.arange(block_len, dtype=jnp.int32)
            key_gate = jnp.transpose(lax.dynamic_slice_in_dim(gathered_gates, offset, block_len, 0))
            updated = []
            for segment, totals_in in zip(segments, state_now):
                query_rows, query_gate, query_pos = segment
                needed = offset <= query_pos[-1]
                advance = partial(
                    attend_block,
                    query_rows=query_rows,
                    query_gate=query_gate,
                    query_pos=query_pos,
                    key_rows=key_rows,
                    value_rows=value_rows,
                    key_gate=key_gate,
                    key_pos=key_pos,
                )
                updated.append(lax.cond(needed, advance, keep_totals, totals_in))
            return tuple(updated)

        return lax.fori_loop(0, key_total // block_len, one_block, state_all)

    return fold_keys


def on_device(
    queries,
    key_vectors,
    value_vectors,
    forget_totals,
    head_gain,
    stream,
    out_weight,
    norm_gain,
    routing,
    route_weights,
    gate_weight,
    up_weight,
    down_weight,
):
    tok_count = queries.shape[0]
    heads_dev = queries.shape[1] // HD
    sp_index = lax.axis_index("sp")
    sp_count = lax.axis_size("sp")
    gathered_gates = lax.all_gather(forget_totals, "sp", axis=0, tiled=True)
    first_pos = sp_index * tok_count
    query_pos = first_pos + jnp.arange(tok_count, dtype=jnp.int32)
    query_gate = jnp.transpose(lax.dynamic_slice_in_dim(gathered_gates, first_pos, tok_count, 0))
    segments = [(queries.reshape(tok_count, heads_dev, HD), query_gate, query_pos)]
    starting = (
        (
            jnp.full((heads_dev, tok_count), masked_score, jnp.float32),
            jnp.zeros((heads_dev, tok_count), jnp.float32),
            jnp.zeros((heads_dev, tok_count, HD), jnp.float32),
        ),
    )
    folder = make_folder(segments, gathered_gates)
    totals = folder(starting, sent_together((key_vectors, value_vectors), "sp", 0, 1), jnp.int32(0))
    run_max, run_sum, run_acc = totals[0]
    attended = run_acc / run_sum[:, :, None]
    inverse_rms = lax.rsqrt(jnp.mean(attended * attended, axis=2, keepdims=True) + 1e-06)
    normed = attended * inverse_rms * head_gain.reshape(heads_dev, 1, HD)
    head_out = (
        jnp.transpose(normed, (1, 0, 2)).reshape(tok_count, heads_dev * HD).astype(jnp.bfloat16)
    )
    token_heads = lax.all_to_all(head_out, "tp", split_axis=0, concat_axis=1, tiled=True)
    mixed_rows = jnp.dot(token_heads, out_weight, preferred_element_type=jnp.float32)
    resid_sum = stream.astype(jnp.float32) + mixed_rows
    center = resid_sum - jnp.mean(resid_sum, axis=1, keepdims=True)
    normed_rows = (
        center * lax.rsqrt(jnp.mean(center * center, axis=1, keepdims=True) + 1e-05) * norm_gain
    ).astype(jnp.bfloat16)
    row_count = normed_rows.shape[0]
    capacity = max(2, 2 * TOP * row_count // sp_count)
    flat_expert = routing.reshape(-1)
    onehot = (flat_expert[:, None] == jnp.arange(sp_count, dtype=jnp.int32)[None, :]).astype(
        jnp.int32
    )
    earlier = jnp.cumsum(onehot, axis=0) - onehot
    slot_index = flat_expert * capacity + jnp.sum(earlier * onehot, axis=1)
    slot_grid = slot_index.reshape(row_count, TOP)
    slot_ids = jnp.arange(sp_count * capacity, dtype=jnp.int32)
    placing = jnp.sum(
        (slot_grid[None, :, :] == slot_ids[:, None, None]).astype(jnp.float32), axis=2
    ).astype(jnp.bfloat16)
    outgoing = jnp.dot(placing, normed_rows, preferred_element_type=jnp.float32).astype(
        jnp.bfloat16
    )
    outgoing = outgoing.reshape(sp_count, capacity, normed_rows.shape[1])
    arrived = lax.all_to_all(outgoing, "sp", split_axis=0, concat_axis=0, tiled=True)
    row_piece = lax.all_gather(arrived.reshape(-1, arrived.shape[2]), "tp", axis=0, tiled=True)
    gate_pre = jnp.dot(row_piece, gate_weight[0], preferred_element_type=jnp.float32)
    up_pre = jnp.dot(row_piece, up_weight[0], preferred_element_type=jnp.float32)
    hidden = (jax.nn.silu(gate_pre) * up_pre).astype(jnp.bfloat16)
    summed = lax.psum_scatter(
        jnp.dot(hidden, down_weight[0], preferred_element_type=jnp.float32).astype(jnp.bfloat16),
        "tp",
        scatter_dimension=0,
        tiled=True,
    )
    expert_out = summed.reshape(sp_count, capacity, -1)
    returned = lax.all_to_all(expert_out, "sp", split_axis=0, concat_axis=0, tiled=True)
    picked = returned.reshape(sp_count * capacity, -1)[slot_index].astype(jnp.float32)
    weighted = picked * route_weights.reshape(-1)[:, None]
    routed = jnp.sum(weighted.reshape(row_count, TOP, -1), axis=1)
    return (resid_sum + routed).astype(jnp.bfloat16)


def solution(mesh):
    in_specs = (
        P("sp", "tp"),
        P("sp", "tp"),
        P("sp", "tp"),
        P("sp", "tp"),
        P("tp"),
        P(("sp", "tp"), None),
        P(),
        P(),
        P(("sp", "tp"), None),
        P(("sp", "tp"), None),
        P("sp", None, "tp"),
        P("sp", None, "tp"),
        P("sp", "tp", None),
    )
    out_specs = P(("sp", "tp"), None)
    return jax.shard_map(
        on_device, mesh=mesh, in_specs=in_specs, out_specs=out_specs, check_vma=False
    )
```

profile of v0, /device:TPU:2, one launch (start us, length us, event | category | flops | bytes accessed | tf_op | source)
XLA Modules:
  0.0 334.1 jit_solution(2829663943095619503)
XLA Ops:
  6.5 1.8 pad_maximum_fusion
  8.3 0.0 all-gather.3.cloned.1.call-update
  8.3 0.8 copy.26
  9.1 0.1 eq.28
  9.2 0.1 fusion.33
  9.3 0.1 reduce_window_sum.11
  9.4 0.2 select_reduce_fusion
  9.6 0.1 reduce_sum.71
  9.7 23.4 %all_gather.10 = f32[8192,1]{0,1:T(1,128)S(1)} all-gather(f32[512,1]{0,1:T(1,128)} %param.20), channel_id=1, replica_groups=mesh['sp'=16,'tp'=16] {'sp'}, dimensions={0}, use_global_device_ids=true | all-gather | bytes 34816 | tf_op jit(solution)/shard_map/all_gather | solution.py:101
  33.1 36.1 %all-gather.3.cloned.1.call-done = bf16[8192,256]{1,0:T(8,128)(2,1)} async-done(((bf16[512,256]{1,0:T(8,128)(2,1)}), bf16[8192,256]{1,0:T(8,128)(2,1)}) %all-gather.3.cloned.1.call-update) | async-done | bytes 4194320 | tf_op jit(solution)/shard_map/all_gather | solution.py:18
  69.2 3.8 %slice_bitcast_fusion = (bf16[8192,1,128]{2,0,1:T(8,128)(2,1)S(1)}, bf16[8192,1,128]{2,0,1:T(8,128)(2,1)}) fusion(bf16[8192,256]{1,0:T(8,128)(2,1)} %all-gather.3.cloned.1.call-done), kind=kLoop, calls=%fused_computation.33 | loop fusion | bytes 8388608 | tf_op jit(solution)/shard_map/reshape | solution.py:52
  73.1 0.0 copy-start.3
  73.1 23.5 %while.17 = (s32[]{:T(128)}, f32[1,512]{1,0:T(1,128)S(1)}, f32[1,512]{1,0:T(1,128)S(1)}, f32[1,512,128]{2,1,0:T(8,128)S(1)}, s32[512]{0:T(512)S(1)}, /*index=5*/...) while((s32[]{:T(128)}, f32[1,512]{1,0:T(1,128)S(1)}, ...), condition=%wide.region_5.6_spmd, body=%wide.region_0.5_spmd.sunk | while | flops 138020352 | bytes 4122969 | solution.py:77
  73.1 0.6 slice.10
  74.3 2.2 conditional.2
  74.3 1.4 fusion.38
  75.7 0.2 fusion.6
  76.0 0.5 fusion.4
  76.5 0.6 slice.10
  77.7 2.2 conditional.2
  77.7 1.4 fusion.38
  79.1 0.2 fusion.6
  79.4 0.5 fusion.4
  79.9 0.6 slice.10
  81.1 0.6 slice.10
  82.3 0.6 slice.10
  83.5 0.6 slice.10
  84.7 0.6 slice.10
  85.9 0.6 slice.10
  87.1 0.6 slice.10
  88.3 0.6 slice.10
  89.5 0.6 slice.10
  90.6 0.6 slice.10
  91.8 0.6 slice.10
  93.0 0.6 slice.10
  94.2 0.6 slice.10
  95.4 0.6 slice.10
  96.6 0.2 multiply_reduce_fusion.2
  96.8 0.9 multiply_convert_fusion.1
  97.7 7.1 %all-to-all-start = ((bf16[16,32,128]{2,1,0:T(8,128)(2,1)}), bf16[16,32,128]{2,1,0:T(8,128)(2,1)S(1)}, u32[]{:S(2)}, u32[]{:S(2)}) async-start(bf16[16,32,128]{2,1,0:T(8,128)(2,1)} %bitcast.16), calls=%async_computation | async-start | bytes 262144 | tf_op jit(solution)/shard_map/all_to_all | solution.py:122
  104.8 0.0 all-gather.5.cloned.1.call-start
  104.9 0.1 copy.28
  105.0 0.1 convert_reduce_fusion
  105.1 0.0 copy-start.1
  105.1 8.4 %all-to-all-done = bf16[16,32,128]{2,1,0:T(8,128)(2,1)S(1)} async-done(((bf16[16,32,128]{2,1,0:T(8,128)(2,1)}), bf16[16,32,128]{2,1,0:T(8,128)(2,1)S(1)}, u32[]{:S(2)}, u32[]{:S(2)}) %all-to-all-start) | async-done | bytes 131104 | tf_op jit(solution)/shard_map/all_to_all | solution.py:122
  113.5 5.0 %fusion.39 = (f32[32]{0:T(128)S(1)}, f32[32,2048]{1,0:T(8,128)S(1)}) fusion(bf16[2048,2048]{1,0:T(8,128)(2,1)} %param.23, bf16[32,2048]{1,0:T(8,128)(2,1)} %param.22, bf16[16,32,128]{2,1,0:T(8,128)(2,1)S(1)} %all-to-all-done), kind=kOutput, calls=%fused_computation.72 | convolution fusion | flops 268632032 | bytes 8913024 | tf_op jit(solution)/shard_map/dot_general | solution.py:123
  118.5 0.2 multiply_reduce_fusion.1
  118.8 0.3 fusion.21
  119.1 46.6 %all_to_all.26 = bf16[16,8,2048]{2,1,0:T(8,128)(2,1)} all-to-all(bf16[16,8,2048]{2,1,0:T(8,128)(2,1)S(1)} %fusion.21), channel_id=1, replica_groups=mesh['sp'=16,'tp'=16] {'sp'}, dimensions={0} | all-to-all | bytes 1048576 | tf_op jit(solution)/shard_map/all_to_all | solution.py:146
  165.8 0.0 all-gather.5.cloned.1.call-update
  165.8 0.0 reduce-scatter.2.cloned.1.call-start
  165.8 49.9 %all-gather.5.cloned.1.call-done = bf16[2048,2048]{1,0:T(8,128)(2,1)} async-done(((bf16[128,2048]{1,0:T(8,128)(2,1)}), bf16[2048,2048]{1,0:T(8,128)(2,1)}) %all-gather.5.cloned.1.call-update) | async-done | bytes 8388624 | tf_op jit(solution)/shard_map/all_gather | solution.py:147
  215.8 7.1 %fusion.25 = f32[2048,256]{1,0:T(8,128)} fusion(bf16[2048,2048]{1,0:T(8,128)(2,1)} %all-gather.5.cloned.1.call-done, bf16[1,2048,256]{2,1,0:T(8,128)(2,1)S(1)} %copy-done.4), kind=kOutput, calls=%fused_computation.37 | convolution fusion | flops 2147483648 | bytes 11534336 | tf_op jit(solution)/shard_map/dot_general | solution.py:148
  222.9 16.8 %convolution_convert_fusion = bf16[2048,2048]{1,0:T(8,128)(2,1)} fusion(bf16[2048,2048]{1,0:T(8,128)(2,1)} %all-gather.5.cloned.1.call-done, f32[2048,256]{1,0:T(8,128)} %fusion.25, bf16[1,256,2048]{2,1,0:T(8,128)(2,1)S(1)} %copy-done, bf16[1,2048,256]{2,1,0:T(8,128)(2,1)} %param.28), kind=kOutput, calls=%fused_computation.27 | convolution fusion | flops 4302307328 | bytes 20971520 | tf_op jit(solution)/shard_map/dot_general | solution.py:152
  239.7 0.0 reduce-scatter.2.cloned.1.call-update
  239.7 69.3 %reduce-scatter.2.cloned.1.call-done = bf16[128,2048]{1,0:T(8,128)(2,1)} async-done(((bf16[2048,2048]{1,0:T(8,128)(2,1)}), bf16[128,2048]{1,0:T(8,128)(2,1)}) %reduce-scatter.2.cloned.1.call-update) | async-done | bytes 524304 | tf_op jit(solution)/shard_map/reduce_scatter | solution.py:151
  309.0 7.3 %all-to-all-start.2 = ((bf16[16,8,2048]{2,1,0:T(8,128)(2,1)}), bf16[16,8,2048]{2,1,0:T(8,128)(2,1)S(1)}, u32[]{:S(2)}, u32[]{:S(2)}) async-start(bf16[16,8,2048]{2,1,0:T(8,128)(2,1)} %bitcast.76), calls=%async_computation.3 | async-start | bytes 1048576 | tf_op jit(solution)/shard_map/all_to_all | solution.py:158
  316.3 0.1 mul.131
  316.4 0.1 copy.29
  316.5 8.6 %all-to-all-done.2 = bf16[16,8,2048]{2,1,0:T(8,128)(2,1)S(1)} async-done(((bf16[16,8,2048]{2,1,0:T(8,128)(2,1)}), bf16[16,8,2048]{2,1,0:T(8,128)(2,1)S(1)}, u32[]{:S(2)}, u32[]{:S(2)}) %all-to-all-start.2) | async-done | bytes 524320 | tf_op jit(solution)/shard_map/all_to_all | solution.py:158
  325.1 0.7 gather_fusion
  325.9 0.3 reshape.179
  326.2 0.7 multiply_reduce_fusion
  326.9 0.7 add_convert_fusion
  (60 shorter events, 0.4 us)
Async XLA Ops:
  6.5 216.3 %copy-start = (bf16[1,256,2048]{2,1,0:T(8,128)(2,1)S(1)}, bf16[1,256,2048]{2,1,0:T(8,128)(2,1)}, u32[]{:S(2)}) copy-start(bf16[1,256,2048]{2,1,0:T(8,128)(2,1)} %param.29) | copy-start | bytes 3145732
  6.5 62.7 %all-gather.3.cloned.1.call-start = ((), (), s32[]{:S(2)}) async-start(), calls=%async_computation.4 | async-start | bytes 4456448 | tf_op jit(solution)/shard_map/all_gather | solution.py:18
  73.1 23.8 %copy-start.3 = (f32[128]{0:T(128)S(1)}, f32[128]{0:T(128)}, u32[]{:S(2)}) copy-start(f32[128]{0:T(128)} %param.21) | copy-start | bytes 1540
  97.7 15.8 %all-to-all-start = ((bf16[16,32,128]{2,1,0:T(8,128)(2,1)}), bf16[16,32,128]{2,1,0:T(8,128)(2,1)S(1)}, u32[]{:S(2)}, u32[]{:S(2)}) async-start(bf16[16,32,128]{2,1,0:T(8,128)(2,1)} %bitcast.16), calls=%async_computation | async-start | bytes 262144 | tf_op jit(solution)/shard_map/all_to_all | solution.py:122
  104.8 110.9 %all-gather.5.cloned.1.call-start = ((), (), s32[]{:S(2)}) async-start(), calls=%async_computation.5 | async-start | bytes 8912896 | tf_op jit(solution)/shard_map/all_gather | solution.py:147
  105.1 13.7 %copy-start.1 = (f32[2048]{0:T(1024)S(1)}, f32[2048]{0:T(1024)}, u32[]{:S(2)}) copy-start(f32[2048]{0:T(1024)} %param.24) | copy-start | bytes 24580
  118.5 97.3 %copy-start.4 = (bf16[1,2048,256]{2,1,0:T(8,128)(2,1)S(1)}, bf16[1,2048,256]{2,1,0:T(8,128)(2,1)}, u32[]{:S(2)}) copy-start(bf16[1,2048,256]{2,1,0:T(8,128)(2,1)} %param.27) | copy-start | bytes 3145732
  165.8 143.2 %reduce-scatter.2.cloned.1.call-start = ((), (), s32[]{:S(2)}) async-start(), calls=%async_computation.6 | async-start | bytes 8912896 | tf_op jit(solution)/shard_map/reduce_scatter | solution.py:151
  239.7 76.8 %copy-start.2 = (f32[32,2]{0,1:T(2,128)S(1)}, f32[32,2]{0,1:T(2,128)}, u32[]{:S(2)}) copy-start(f32[32,2]{0,1:T(2,128)} %param.26) | copy-start | bytes 772
  309.0 16.1 %all-to-all-start.2 = ((bf16[16,8,2048]{2,1,0:T(8,128)(2,1)}), bf16[16,8,2048]{2,1,0:T(8,128)(2,1)S(1)}, u32[]{:S(2)}, u32[]{:S(2)}) async-start(bf16[16,8,2048]{2,1,0:T(8,128)(2,1)} %bitcast.76), calls=%async_computation.3 | async-start | bytes 1048576 | tf_op jit(solution)/shard_map/all_to_all | solution.py:158
Sparse Core Ops, SparseCore 0:
  9.8 59.4 all-gather.2
  165.9 49.8 all-gather.4
  239.8 69.1 reduce-scatter.1
where the time goes:
time: 335 us; the launch traced here: 334 us
  waiting for transfers between devices  172 us (51%)
  blocking collectives  70.1 us (21%)
  matrix products  33 us (10%)
  local copies, waits for them, and re-layouts  15.5 us (5%)
  starting transfers between devices  14.5 us (4%)
  between operations  13.3 us (4%)
  loops' own time  9.92 us (3%)
  other arithmetic  5.49 us (2%)
    reduce_scatter x1, waiting for transfers between devices, on_device(): lax.psum_scatter(jnp.dot(hidden, down_weight[0], preferred_element_type=j...  69.3 us
    all_gather x1, waiting for transfers between devices, on_device(): lax.all_gather(arrived.reshape(-1, arrived.shape[2]), 'tp', axis=0, tiled...  49.9 us
    all_to_all x1, blocking collectives, on_device(): lax.all_to_all(outgoing, 'sp', split_axis=0, concat_axis=0, tiled=True)  46.6 us
    all_gather x1, waiting for transfers between devices, sent_together(): lax.all_gather(both, axis, axis=dim, tiled=True)  36.1 us
    all_gather x1, blocking collectives, on_device(): gathered_gates = lax.all_gather(forget_totals, 'sp', axis=0, tiled=True)  23.4 us
    dot_general x1, matrix products, on_device(): jnp.dot(hidden, down_weight[0], preferred_element_type=jnp.float32)  16.8 us
    another operation x1, loops' own time, fold_keys(): return lax.fori_loop(0, key_total // block_len, one_block, state_all)  9.6 us
    slice x16, local copies, waits for them, and re-layouts, one_block(): needed = offset <= query_pos[-1]  9.2 us
  transfers between devices with their start and end apart: 5, of which 5 were waited for; matrix products, arithmetic and copies ran while one was open for 1% of the time, Pallas kernels for 0%

commit v1 on v0

--- a/solution.py
+++ b/solution.py
@@ -144,7 +144,9 @@
     )
     outgoing = outgoing.reshape(sp_count, capacity, normed_rows.shape[1])
     arrived = lax.all_to_all(outgoing, "sp", split_axis=0, concat_axis=0, tiled=True)
-    row_piece = lax.all_gather(arrived.reshape(-1, arrived.shape[2]), "tp", axis=0, tiled=True)
+    x = arrived.reshape(-1, arrived.shape[2])
+    copies = jnp.concatenate([x] * lax.axis_size("tp"), axis=0)
+    row_piece = lax.all_to_all(copies, "tp", 0, 0, tiled=True)
     gate_pre = jnp.dot(row_piece, gate_weight[0], preferred_element_type=jnp.float32)
     up_pre = jnp.dot(row_piece, up_weight[0], preferred_element_type=jnp.float32)
     hidden = (jax.nn.silu(gate_pre) * up_pre).astype(jnp.bfloat16)

time: 335 us -> 471 us (1.41)
  blocking collectives: 70.1 us -> 257 us
  waiting for transfers between devices: 172 us -> 120 us
    all_to_all x0 -> x1, blocking collectives: none -> 187 us  [on_device(): row_piece = lax.all_to_all(copies, 'tp', 0, 0, tiled=True)]
    all_gather x1 -> x0, waiting for transfers between devices: 49.9 us -> none  [on_device(): lax.all_gather(arrived.reshape(-1, arrived.shape[2]), 'tp', axis=0, tiled...]
  transfers between devices with their start and end apart: 5 -> 4, of which waited for: 5 -> 4; matrix products, arithmetic and copies ran while one was open for 1% -> 0% of each run, Pallas kernels for 0% -> 0%
where the time goes in v1:
time: 471 us; the launch traced here: 470 us
  blocking collectives  257 us (55%)
  waiting for transfers between devices  120 us (25%)
  matrix products  29.8 us (6%)
  local copies, waits for them, and re-layouts  19.3 us (4%)
  starting transfers between devices  14.4 us (3%)
  between operations  13.7 us (3%)
  loops' own time  9.92 us (2%)
  other arithmetic  5.5 us (1%)
    all_to_all x1, blocking collectives, on_device(): row_piece = lax.all_to_all(copies, 'tp', 0, 0, tiled=True)  187 us
    reduce_scatter x1, waiting for transfers between devices, on_device(): lax.psum_scatter(jnp.dot(hidden, down_weight[0], preferred_element_type=j...  66.7 us
    all_to_all x1, blocking collectives, on_device(): lax.all_to_all(outgoing, 'sp', split_axis=0, concat_axis=0, tiled=True)  46.6 us
    all_gather x1, waiting for transfers between devices, sent_together(): lax.all_gather(both, axis, axis=dim, tiled=True)  36.1 us
    all_gather x1, blocking collectives, on_device(): gathered_gates = lax.all_gather(forget_totals, 'sp', axis=0, tiled=True)  23.4 us
    dot_general x1, matrix products, on_device(): jnp.dot(hidden, down_weight[0], preferred_element_type=jnp.float32)  16.8 us
    another operation x1, loops' own time, fold_keys(): return lax.fori_loop(0, key_total // block_len, one_block, state_all)  9.6 us
  transfers between devices with their start and end apart: 4, of which 4 were waited for; matrix products, arithmetic and copies ran while one was open for 0% of the time, Pallas kernels for 0%

profile of v1, /device:TPU:2, one launch (start us, length us, event | category | flops | bytes accessed | tf_op | source)
XLA Modules:
  0.0 469.7 jit_solution(1226308253965401262)
XLA Ops:
  6.5 1.8 pad_maximum_fusion
  8.3 0.0 all-gather.2.cloned.1.call-update
  8.3 0.8 copy.26
  9.1 0.1 eq.28
  9.2 0.1 fusion.33
  9.3 0.1 reduce_window_sum.11
  9.4 0.2 select_reduce_fusion
  9.6 0.1 reduce_sum.71
  9.7 23.4 %all_gather.7 = f32[8192,1]{0,1:T(1,128)S(1)} all-gather(f32[512,1]{0,1:T(1,128)} %param.20), channel_id=1, replica_groups=mesh['sp'=16,'tp'=16] {'sp'}, dimensions={0}, use_global_device_ids=true | all-gather | bytes 34816 | tf_op jit(solution)/shard_map/all_gather | solution.py:101
  33.1 36.1 %all-gather.2.cloned.1.call-done = bf16[8192,256]{1,0:T(8,128)(2,1)} async-done(((bf16[512,256]{1,0:T(8,128)(2,1)}), bf16[8192,256]{1,0:T(8,128)(2,1)}) %all-gather.2.cloned.1.call-update) | async-done | bytes 4194320 | tf_op jit(solution)/shard_map/all_gather | solution.py:18
  69.2 3.8 slice_bitcast_fusion
  73.1 0.0 copy-start.4
  73.1 23.5 %while.17 = (s32[]{:T(128)}, f32[1,512]{1,0:T(1,128)S(1)}, f32[1,512]{1,0:T(1,128)S(1)}, f32[1,512,128]{2,1,0:T(8,128)S(1)}, s32[512]{0:T(512)S(1)}, /*index=5*/...) while((s32[]{:T(128)}, f32[1,512]{1,0:T(1,128)S(1)}, ...), condition=%wide.region_5.6_spmd, body=%wide.region_0.5_spmd.sunk | while | flops 138020352 | bytes 4122969 | solution.py:77
  73.1 0.6 slice.10
  74.3 2.2 conditional.2
  74.3 1.4 fusion.38
  75.7 0.2 fusion.6
  76.0 0.5 fusion.4
  76.5 0.6 slice.10
  77.7 2.2 conditional.2
  77.7 1.4 fusion.38
  79.1 0.2 fusion.6
  79.4 0.5 fusion.4
  79.9 0.6 slice.10
  81.1 0.6 slice.10
  82.3 0.6 slice.10
  83.5 0.6 slice.10
  84.7 0.6 slice.10
  85.9 0.6 slice.10
  87.1 0.6 slice.10
  88.3 0.6 slice.10
  89.5 0.6 slice.10
  90.6 0.6 slice.10
  91.8 0.6 slice.10
  93.0 0.6 slice.10
  94.2 0.6 slice.10
  95.4 0.6 slice.10
  96.6 0.2 multiply_reduce_fusion.2
  96.8 0.9 multiply_convert_fusion.1
  97.7 7.1 %all-to-all-start = ((bf16[16,32,128]{2,1,0:T(8,128)(2,1)}), bf16[16,32,128]{2,1,0:T(8,128)(2,1)S(1)}, u32[]{:S(2)}, u32[]{:S(2)}) async-start(bf16[16,32,128]{2,1,0:T(8,128)(2,1)} %bitcast.16), calls=%async_computation | async-start | bytes 262144 | tf_op jit(solution)/shard_map/all_to_all | solution.py:122
  104.8 0.0 copy-start.2
  104.8 0.0 reduce-scatter.2.cloned.1.call-start
  104.9 0.1 copy.28
  105.0 0.1 convert_reduce_fusion
  105.1 8.4 %all-to-all-done = bf16[16,32,128]{2,1,0:T(8,128)(2,1)S(1)} async-done(((bf16[16,32,128]{2,1,0:T(8,128)(2,1)}), bf16[16,32,128]{2,1,0:T(8,128)(2,1)S(1)}, u32[]{:S(2)}, u32[]{:S(2)}) %all-to-all-start) | async-done | bytes 131104 | tf_op jit(solution)/shard_map/all_to_all | solution.py:122
  113.5 5.0 %fusion.39 = (f32[32]{0:T(128)S(1)}, f32[32,2048]{1,0:T(8,128)S(1)}) fusion(bf16[2048,2048]{1,0:T(8,128)(2,1)} %param.23, bf16[32,2048]{1,0:T(8,128)(2,1)} %param.22, bf16[16,32,128]{2,1,0:T(8,128)(2,1)S(1)} %all-to-all-done), kind=kOutput, calls=%fused_computation.88 | convolution fusion | flops 268632032 | bytes 8913024 | tf_op jit(solution)/shard_map/dot_general | solution.py:123
  118.5 0.2 multiply_reduce_fusion.1
  118.8 0.3 fusion.21
  119.1 46.6 %all_to_all.38 = bf16[16,8,2048]{2,1,0:T(8,128)(2,1)S(1)} all-to-all(bf16[16,8,2048]{2,1,0:T(8,128)(2,1)S(1)} %fusion.21), channel_id=1, replica_groups=mesh['sp'=16,'tp'=16] {'sp'}, dimensions={0} | all-to-all | bytes 1048576 | tf_op jit(solution)/shard_map/all_to_all | solution.py:146
  166.5 0.0 copy-start.5
  166.5 187.3 %all_to_all.39 = bf16[16,128,2048]{2,1,0:T(8,128)(2,1)S(1)} all-to-all(bf16[16,128,2048]{2,1,0:T(8,128)(2,1)S(1)} %bitcast.91), channel_id=1, replica_groups=mesh['sp'=16,'tp'=16] {'tp'}, dimensions={0} | all-to-all | bytes 16777216 | tf_op jit(solution)/shard_map/all_to_all | solution.py:149
  353.7 3.2 copy-done.1
  357.0 3.8 fusion.25
  360.7 16.8 %convolution_convert_fusion = bf16[2048,2048]{1,0:T(8,128)(2,1)} fusion(bf16[2048,2048]{1,0:T(8,128)(2,1)} %bitcast.93, f32[2048,256]{1,0:T(8,128)} %fusion.25, bf16[1,256,2048]{2,1,0:T(8,128)(2,1)S(1)} %copy-done, bf16[1,2048,256]{2,1,0:T(8,128)(2,1)} %param.28), kind=kOutput, calls=%fused_computation.27 | convolution fusion | flops 4302307328 | bytes 20971520 | tf_op jit(solution)/shard_map/dot_general | solution.py:154
  377.6 0.0 reduce-scatter.2.cloned.1.call-update
  377.6 66.7 %reduce-scatter.2.cloned.1.call-done = bf16[128,2048]{1,0:T(8,128)(2,1)} async-done(((bf16[2048,2048]{1,0:T(8,128)(2,1)}), bf16[128,2048]{1,0:T(8,128)(2,1)}) %reduce-scatter.2.cloned.1.call-update) | async-done | bytes 524304 | tf_op jit(solution)/shard_map/reduce_scatter | solution.py:153
  444.3 7.3 %all-to-all-start.3 = ((bf16[16,8,2048]{2,1,0:T(8,128)(2,1)}), bf16[16,8,2048]{2,1,0:T(8,128)(2,1)S(1)}, u32[]{:S(2)}, u32[]{:S(2)}) async-start(bf16[16,8,2048]{2,1,0:T(8,128)(2,1)} %bitcast.96), calls=%async_computation.4 | async-start | bytes 1048576 | tf_op jit(solution)/shard_map/all_to_all | solution.py:160
  451.6 0.1 mul.131
  451.7 0.1 copy.29
  451.8 8.6 %all-to-all-done.3 = bf16[16,8,2048]{2,1,0:T(8,128)(2,1)S(1)} async-done(((bf16[16,8,2048]{2,1,0:T(8,128)(2,1)}), bf16[16,8,2048]{2,1,0:T(8,128)(2,1)S(1)}, u32[]{:S(2)}, u32[]{:S(2)}) %all-to-all-start.3) | async-done | bytes 524320 | tf_op jit(solution)/shard_map/all_to_all | solution.py:160
  460.3 0.7 gather_fusion
  461.1 0.3 reshape.181
  461.4 0.7 multiply_reduce_fusion
  462.2 0.7 add_convert_fusion
  (76 shorter events, 1.1 us)
Async XLA Ops:
  6.5 354.2 %copy-start = (bf16[1,256,2048]{2,1,0:T(8,128)(2,1)S(1)}, bf16[1,256,2048]{2,1,0:T(8,128)(2,1)}, u32[]{:S(2)}) copy-start(bf16[1,256,2048]{2,1,0:T(8,128)(2,1)} %param.29) | copy-start | bytes 3145732
  6.5 62.7 %all-gather.2.cloned.1.call-start = ((), (), s32[]{:S(2)}) async-start(), calls=%async_computation.5 | async-start | bytes 4456448 | tf_op jit(solution)/shard_map/all_gather | solution.py:18
  73.1 23.8 %copy-start.4 = (f32[128]{0:T(128)S(1)}, f32[128]{0:T(128)}, u32[]{:S(2)}) copy-start(f32[128]{0:T(128)} %param.21) | copy-start | bytes 1540
  97.7 15.8 %all-to-all-start = ((bf16[16,32,128]{2,1,0:T(8,128)(2,1)}), bf16[16,32,128]{2,1,0:T(8,128)(2,1)S(1)}, u32[]{:S(2)}, u32[]{:S(2)}) async-start(bf16[16,32,128]{2,1,0:T(8,128)(2,1)} %bitcast.16), calls=%async_computation | async-start | bytes 262144 | tf_op jit(solution)/shard_map/all_to_all | solution.py:122
  104.8 13.9 %copy-start.2 = (f32[2048]{0:T(1024)S(1)}, f32[2048]{0:T(1024)}, u32[]{:S(2)}) copy-start(f32[2048]{0:T(1024)} %param.24) | copy-start | bytes 24580
  104.8 339.4 %reduce-scatter.2.cloned.1.call-start = ((), (), s32[]{:S(2)}) async-start(), calls=%async_computation.6 | async-start | bytes 8912896 | tf_op jit(solution)/shard_map/reduce_scatter | solution.py:153
  166.5 190.5 %copy-start.5 = (bf16[1,2048,256]{2,1,0:T(8,128)(2,1)S(1)}, bf16[1,2048,256]{2,1,0:T(8,128)(2,1)}, u32[]{:S(2)}) copy-start(bf16[1,2048,256]{2,1,0:T(8,128)(2,1)} %param.27) | copy-start | bytes 3145732
  353.7 3.2 copy-start.1
  377.6 74.1 %copy-start.3 = (f32[32,2]{0,1:T(2,128)S(1)}, f32[32,2]{0,1:T(2,128)}, u32[]{:S(2)}) copy-start(f32[32,2]{0,1:T(2,128)} %param.26) | copy-start | bytes 772
  444.3 16.1 %all-to-all-start.3 = ((bf16[16,8,2048]{2,1,0:T(8,128)(2,1)}), bf16[16,8,2048]{2,1,0:T(8,128)(2,1)S(1)}, u32[]{:S(2)}, u32[]{:S(2)}) async-start(bf16[16,8,2048]{2,1,0:T(8,128)(2,1)} %bitcast.96), calls=%async_computation.4 | async-start | bytes 1048576 | tf_op jit(solution)/shard_map/all_to_all | solution.py:160
Sparse Core Ops, SparseCore 0:
  9.8 59.4 all-gather.1
  377.7 66.4 reduce-scatter.1
